TPU v7x, 512 devices: a whole 4x8x8 slice. The times are simulated.
512 devices in a mesh: fs: 128 (over z, y, core), tp: 4 (over x).
Axes of the slice: x: 4, y: 8, z: 8, core: 2. Of those that a mesh axis runs over, the one named last changes fastest.
Arguments:
- prompt_tokens: bfloat16 [768, 4096], P('tp'), may hold values from -6 to 6
- norm_gain: float32 [4096], P('fs'), may hold values from 0.1 to 1.9
- gate_trained: float32 [4096, 11264], P('fs', 'tp'), may hold values from -0.09375 to 0.09375
- up_trained: float32 [4096, 11264], P('fs', 'tp'), may hold values from -0.09375 to 0.09375
- down_trained: float32 [11264, 4096], P('fs', 'tp'), may hold values from -0.21875 to 0.21875
Outputs:
- gate_serving: bfloat16 [4096, 11264], P(None, 'fs')
- up_serving: bfloat16 [4096, 11264], P(None, 'fs')
- down_serving: bfloat16 [11264, 4096], P('fs')
- mixed: bfloat16 [768, 4096], P('tp', 'fs')
All inputs are finite; a program needn't handle non-finite values.
Results may differ from a plain program's by a relative error of at most 0.0082.
Values may be sent and summed in bfloat16 or wider, within the bound.
A program may use at most 64 MiB of HBM per device.

v0:
```python
import jax
import jax.numpy as jnp
from jax import lax
from jax.sharding import Mesh
from jax.sharding import PartitionSpec as P

FS = ("fs_0", "fs_1", "fs_2")


def copy_for_each(array, axis):
    peers = lax.axis_size(axis)
    return lax.all_to_all(
        jnp.broadcast_to(array[None], (peers, *array.shape)), axis, 0, 0, tiled=True
    )


def laid_out(pieces, dim):
    pieces = jnp.moveaxis(pieces, 0, dim)
    lengths = pieces.shape
    return pieces.reshape(*lengths[:dim], lengths[dim] * lengths[dim + 1], *lengths[dim + 2 :])


def gather_directly(array, axis, dim):
    pieces = copy_for_each(array, axis)
    return laid_out(pieces, dim)


def in_one_piece(arrays, axis, dim, along):
    widths = [a.shape[along] for a in arrays]
    both = jnp.concatenate(arrays, axis=along)
    whole = gather_directly(both, axis, dim)
    return tuple(jnp.split(whole, [sum(widths[:k]) for k in range(1, len(widths))], axis=along))


def sum_in_order(pieces, axes, sequence):
    inside = pieces.shape[1:]
    pieces = pieces.reshape(*(lax.axis_size(a) for a in axes), *inside)
    pieces = jnp.moveaxis(pieces, sequence, range(len(axes))).reshape(-1, *inside)
    for k in sequence:
        pieces = lax.psum_scatter(pieces, axes[k], scatter_dimension=0, tiled=True)
    return pieces[0]


def in_blocks(array, dim, peers):
    lengths = array.shape
    pieces = array.reshape(*lengths[:dim], peers, lengths[dim] // peers, *lengths[dim + 1 :])
    return jnp.moveaxis(pieces, dim, 0)


def scatter_axes(array, axes, sequence, dim):
    peers = lax.axis_size(axes)
    return sum_in_order(in_blocks(array, dim, peers), axes, sequence)


def on_device(prompt_tokens, norm_gain, gate_trained, up_trained, down_trained):
    fs_count = lax.axis_size(FS)
    gate_cast = (gate_trained * norm_gain[:, None]).astype(jnp.bfloat16)
    up_cast = (up_trained * norm_gain[:, None]).astype(jnp.bfloat16)
    down_cast = down_trained.astype(jnp.bfloat16)
    down_serving = lax.all_gather(down_cast, "tp", axis=1, tiled=True)
    gate_part, up_part = (
        lax.all_to_all(gate_cast, "tp", split_axis=0, concat_axis=1, tiled=True),
        lax.all_to_all(up_cast, "tp", split_axis=0, concat_axis=1, tiled=True),
    )
    gate_mid, up_mid = (
        lax.all_to_all(gate_part, FS, split_axis=1, concat_axis=0, tiled=True),
        lax.all_to_all(up_part, FS, split_axis=1, concat_axis=0, tiled=True),
    )
    share = gate_mid.shape[0] // fs_count
    width = gate_mid.shape[1]
    gate_blocks, up_blocks = in_one_piece(
        (gate_mid.reshape(fs_count, share, width), up_mid.reshape(fs_count, share, width)),
        "tp",
        1,
        0,
    )
    gate_serving = gate_blocks.reshape(-1, width)
    up_serving = up_blocks.reshape(-1, width)
    tokens = prompt_tokens.astype(jnp.float32)
    scale = lax.rsqrt(jnp.mean(tokens * tokens, axis=-1, keepdims=True) + 1e-06)
    normed = (tokens * scale).astype(jnp.bfloat16)
    contract = (((0,), (1,)), ((), ()))
    gate_cols = lax.dot_general(gate_serving, normed, contract, preferred_element_type=jnp.float32)
    up_cols = lax.dot_general(up_serving, normed, contract, preferred_element_type=jnp.float32)
    hidden_cols = (jax.nn.silu(gate_cols) * up_cols).astype(jnp.bfloat16)
    summed = scatter_axes(
        lax.dot_general(
            down_serving, hidden_cols, (((0,), (0,)), ((), ())), preferred_element_type=jnp.float32
        ),
        FS,
        (2, 0, 1),
        0,
    )
    mixed = summed.T.astype(jnp.bfloat16)
    return (gate_serving, up_serving, down_serving, mixed)


def solution(mesh):
    finer = Mesh(mesh.devices.reshape(8, 8, 2, mesh.shape["tp"]), ("fs_0", "fs_1", "fs_2", "tp"))
    return jax.shard_map(
        on_device,
        mesh=finer,
        in_specs=(P("tp", None), P(FS), P(FS, "tp"), P(FS, "tp"), P(FS, "tp")),
        out_specs=(P(None, FS), P(None, FS), P(FS, None), P("tp", FS)),
        check_vma=False,
    )
```

profile of v0, /device:TPU:2, one launch (start us, length us, event | category | flops | bytes accessed | tf_op | source)
XLA Modules:
  0.0 245.4 jit_solution(9093493141766342540)
XLA Ops:
  7.2 1.9 fusion.7
  9.1 13.0 %all_to_all.69 = bf16[4,8,2816]{2,1,0:T(8,128)(2,1)S(1)} all-to-all(bf16[4,8,2816]{2,1,0:T(8,128)(2,1)S(1)} %get-tuple-element.19), channel_id=1, replica_groups=mesh['fs_0'=8,'fs_1'=8,'fs_2'=2,'tp'=4] {'tp'}, dimensions={0} | all-to-all | bytes 360448 | tf_op jit(solution)/shard_map/all_to_all | solution.py:63
  22.1 4.8 %all-to-all-start = ((bf16[4,8,2816]{2,1,0:T(8,128)(2,1)}), bf16[4,8,2816]{2,1,0:T(8,128)(2,1)S(1)}, u32[]{:S(2)}, u32[]{:S(2)}) async-start(bf16[4,8,2816]{2,1,0:T(8,128)(2,1)} %get-tuple-element.18), calls=%async_computation | async-start | bytes 360448 | tf_op jit(solution)/shard_map/all_to_all | solution.py:62
  26.9 0.6 all_to_all.60
  27.5 0.9 copy.26
  28.4 3.2 %all-to-all-done = bf16[4,8,2816]{2,1,0:T(8,128)(2,1)S(1)} async-done(((bf16[4,8,2816]{2,1,0:T(8,128)(2,1)}), bf16[4,8,2816]{2,1,0:T(8,128)(2,1)S(1)}, u32[]{:S(2)}, u32[]{:S(2)}) %all-to-all-start) | async-done | bytes 180256 | tf_op jit(solution)/shard_map/all_to_all | solution.py:62
  31.6 14.2 %all-to-all-start.3 = ((bf16[8,128,88]{2,0,1:T(8,128)(2,1)}), bf16[8,128,88]{2,0,1:T(8,128)(2,1)S(1)}, u32[]{:S(2)}, u32[]{:S(2)}) async-start(bf16[8,128,88]{2,0,1:T(8,128)(2,1)} %copy.26), calls=%async_computation.3 | async-start | bytes 524288 | tf_op jit(solution)/shard_map/all_to_all | solution.py:67
  45.9 0.6 all_to_all.54
  46.5 0.2 copy.24
  46.7 13.8 %all-to-all-done.3 = bf16[8,128,88]{2,0,1:T(8,128)(2,1)S(1)} async-done(((bf16[8,128,88]{2,0,1:T(8,128)(2,1)}), bf16[8,128,88]{2,0,1:T(8,128)(2,1)S(1)}, u32[]{:S(2)}, u32[]{:S(2)}) %all-to-all-start.3) | async-done | bytes 180256 | tf_op jit(solution)/shard_map/all_to_all | solution.py:67
  60.6 20.2 %all_to_all.70 = bf16[8,128,88]{2,0,1:T(8,128)(2,1)S(1)} all-to-all(bf16[8,128,88]{2,0,1:T(8,128)(2,1)S(1)} %copy.24), channel_id=1, replica_groups=mesh['fs_0'=8,'fs_1'=8,'fs_2'=2,'tp'=4] {'fs_0','fs_1','fs_2'}, dimensions={1} | all-to-all | bytes 360448 | tf_op jit(solution)/shard_map/all_to_all | solution.py:66
  80.8 0.1 pad_maximum_fusion
  80.9 0.3 copy.27
  81.2 1.2 broadcast_in_dim.2
  82.4 5.1 %all-to-all-start.4 = ((bf16[4,256,8,88]{1,3,2,0:T(8,128)(2,1)}), bf16[4,256,8,88]{1,3,2,0:T(8,128)(2,1)S(1)}, u32[]{:S(2)}, u32[]{:S(2)}) async-start(bf16[4,256,8,88]{1,3,2,0:T(8,128)(2,1)} %broadcast_in_dim.2), calls=%async_computation.4 | async-start | bytes 2883584 | tf_op jit(solution)/shard_map/all_to_all | solution.py:12
  87.6 0.4 fusion
  88.0 26.8 %all_gather.3 = bf16[88,4096]{1,0:T(8,128)(2,1)} all-gather(bf16[88,1024]{1,0:T(8,128)(2,1)S(1)} %convert_element_type.29), channel_id=1, replica_groups=mesh['fs_0'=8,'fs_1'=8,'fs_2'=2,'tp'=4] {'tp'}, dimensions={1}, use_global_device_ids=true | all-gather | bytes 901120 | tf_op jit(solution)/shard_map/all_gather | solution.py:60
  114.8 1.4 fusion.16
  116.1 2.7 %copy.29 = bf16[128,4,8,88]{3,2,1,0:T(8,128)(2,1)} copy(bf16[128,4,8,88]{0,3,2,1:T(8,128)(2,1)} %get-tuple-element.16) | data formatting | bytes 1441792 | tf_op jit(solution)/shard_map/split | solution.py:32
  118.8 0.9 copy.28
  119.8 0.7 fusion.5
  120.5 0.3 copy-done.3
  120.8 4.0 %convolution_bitcast_fusion = f32[4096,192]{0,1:T(8,128)S(1)} fusion(bf16[88,4096]{1,0:T(8,128)(2,1)} %all_gather.3, bf16[4096,88]{1,0:T(8,128)(2,1)} %bitcast.26, bf16[192,4096]{1,0:T(8,128)(2,1)} %param.5, f32[192]{0:T(256)S(1)} %add_rsqrt_fusion, f32[88,192]{1,0:T(8,128)S(1)} %fusion.5), kind=kOutput, calls=%fused_computation | convolution fusion | flops 279284736 | bytes 6228736 | tf_op jit(solution)/shard_map/dot_general | solution.py:87
  124.8 3.4 %copy.30 = f32[4096,192]{1,0:T(8,128)} copy(f32[4096,192]{0,1:T(8,128)S(1)} %convolution_bitcast_fusion) | data formatting | bytes 6291456 | tf_op jit(solution)/shard_map/dot_general | solution.py:87
  128.2 4.7 %copy.31 = f32[2,8,8,32,192]{4,3,2,1,0:T(8,128)} copy(f32[2,8,8,32,192]{4,3,0,2,1:T(8,128)} %bitcast.24) | data formatting | bytes 6291456 | tf_op jit(solution)/shard_map/transpose | solution.py:38
  133.0 13.1 %reduce-scatter.4.cloned.1.call-done = f32[64,32,192]{2,1,0:T(8,128)} async-done(((f32[128,32,192]{2,1,0:T(8,128)}), f32[64,32,192]{2,1,0:T(8,128)}) %reduce-scatter.4.cloned.1.call-update) | async-done | bytes 1572880 | tf_op jit(solution)/shard_map/reduce_scatter | solution.py:40
  146.2 50.0 %reduce-scatter.6.cloned.1.call-done = f32[8,32,192]{2,1,0:T(8,128)} async-done(((f32[64,32,192]{2,1,0:T(8,128)}), f32[8,32,192]{2,1,0:T(8,128)}) %reduce-scatter.6.cloned.1.call-update) | async-done | bytes 196624 | tf_op jit(solution)/shard_map/reduce_scatter | solution.py:40
  196.2 1.2 copy.33
  197.5 1.2 copy.32
  198.7 38.0 %reduce-scatter.8.cloned.1.call-done = f32[1,32,192]{2,1,0:T(8,128)} async-done(((f32[8,32,192]{2,1,0:T(8,128)}), f32[1,32,192]{2,1,0:T(8,128)}) %reduce-scatter.8.cloned.1.call-update) | async-done | bytes 24592 | tf_op jit(solution)/shard_map/reduce_scatter | solution.py:40
  236.7 1.4 convert_bitcast_fusion
  238.0 0.9 copy.35
  (24 shorter events, 0.3 us)
Async XLA Ops:
  22.1 9.6 %all-to-all-start = ((bf16[4,8,2816]{2,1,0:T(8,128)(2,1)}), bf16[4,8,2816]{2,1,0:T(8,128)(2,1)S(1)}, u32[]{:S(2)}, u32[]{:S(2)}) async-start(bf16[4,8,2816]{2,1,0:T(8,128)(2,1)} %get-tuple-element.18), calls=%async_computation | async-start | bytes 360448 | tf_op jit(solution)/shard_map/all_to_all | solution.py:62
  31.6 28.9 %all-to-all-start.3 = ((bf16[8,128,88]{2,0,1:T(8,128)(2,1)}), bf16[8,128,88]{2,0,1:T(8,128)(2,1)S(1)}, u32[]{:S(2)}, u32[]{:S(2)}) async-start(bf16[8,128,88]{2,0,1:T(8,128)(2,1)} %copy.26), calls=%async_computation.3 | async-start | bytes 524288 | tf_op jit(solution)/shard_map/all_to_all | solution.py:67
  82.4 5.1 %copy-start.6 = (f32[88,1024]{1,0:T(8,128)S(1)}, f32[88,1024]{1,0:T(8,128)}, u32[]{:S(2)}) copy-start(f32[88,1024]{1,0:T(8,128)} %param.9) | copy-start | bytes 1081348
  82.4 5.1 %copy-start.2 = (bf16[192,4096]{1,0:T(8,128)(2,1)S(1)}, bf16[192,4096]{1,0:T(8,128)(2,1)}, u32[]{:S(2)}) copy-start(bf16[192,4096]{1,0:T(8,128)(2,1)} %param.5) | copy-start | bytes 4718596
  82.4 32.3 %all-to-all-start.4 = ((bf16[4,256,8,88]{1,3,2,0:T(8,128)(2,1)}), bf16[4,256,8,88]{1,3,2,0:T(8,128)(2,1)S(1)}, u32[]{:S(2)}, u32[]{:S(2)}) async-start(bf16[4,256,8,88]{1,3,2,0:T(8,128)(2,1)} %broadcast_in_dim.2), calls=%async_computation.4 | async-start | bytes 2883584 | tf_op jit(solution)/shard_map/all_to_all | solution.py:12
  87.5 58.6 %reduce-scatter.4.cloned.1.call-start = ((), (), s32[]{:S(2)}) async-start(), calls=%async_computation.8 | async-start | bytes 6291456 | tf_op jit(solution)/shard_map/reduce_scatter | solution.py:40
  116.1 2.7 %copy-start.5 = (bf16[128,4,8,88]{0,3,2,1:T(8,128)(2,1)S(1)}, bf16[128,4,8,88]{0,3,2,1:T(8,128)(2,1)}, u32[]{:S(2)}) copy-start(bf16[128,4,8,88]{0,3,2,1:T(8,128)(2,1)} %get-tuple-element.17) | copy-start | bytes 2162692
  119.8 1.1 copy-start.3
  132.9 63.3 %copy-start = (bf16[128,4,8,88]{3,2,1,0:T(8,128)(2,1)S(1)}, bf16[128,4,8,88]{3,2,1,0:T(8,128)(2,1)}, u32[]{:S(2)}) copy-start(bf16[128,4,8,88]{3,2,1,0:T(8,128)(2,1)} %copy.29) | copy-start | bytes 2162692
  132.9 63.3 %reduce-scatter.6.cloned.1.call-start = ((), (), s32[]{:S(2)}) async-start(), calls=%async_computation.9 | async-start | bytes 2359296 | tf_op jit(solution)/shard_map/reduce_scatter | solution.py:40
  146.1 51.4 %copy-start.4 = (bf16[128,4,8,88]{3,2,1,0:T(8,128)(2,1)S(1)}, bf16[128,4,8,88]{3,2,1,0:T(8,128)(2,1)}, u32[]{:S(2)}) copy-start(bf16[128,4,8,88]{3,2,1,0:T(8,128)(2,1)} %copy-done.3) | copy-start | bytes 2162692
  146.1 90.5 %reduce-scatter.8.cloned.1.call-start = ((), (), s32[]{:S(2)}) async-start(), calls=%async_computation.10 | async-start | bytes 294912 | tf_op jit(solution)/shard_map/reduce_scatter | solution.py:40
  196.2 41.8 %copy-start.1 = (bf16[88,4096]{1,0:T(8,128)(2,1)S(1)}, bf16[88,4096]{1,0:T(8,128)(2,1)}, u32[]{:S(2)}) copy-start(bf16[88,4096]{1,0:T(8,128)(2,1)} %all_gather.3) | copy-start | bytes 2162692
Sparse Core Ops, SparseCore 0:
  133.0 13.0 reduce-scatter.3
  148.9 47.2 reduce-scatter.5
  199.0 37.6 reduce-scatter.7
where the time goes:
time: 246 us; the launch traced here: 245 us
  waiting for transfers between devices  118 us (48%)
  blocking collectives  60 us (24%)
  starting transfers between devices  24.2 us (10%)
  local copies, waits for them, and re-layouts  20.7 us (8%)
  between operations  13.9 us (6%)
  matrix products  4.66 us (2%)
  other arithmetic  3.78 us (2%)
    reduce_scatter x3, waiting for transfers between devices, sum_in_order(): pieces = lax.psum_scatter(pieces, axes[k], scatter_dimension=0, tiled=True)  101 us
    all_gather x1, blocking collectives, on_device(): down_serving = lax.all_gather(down_cast, 'tp', axis=1, tiled=True)  26.8 us
    all_to_all x1, blocking collectives, on_device(): lax.all_to_all(gate_part, FS, split_axis=1, concat_axis=0, tiled=True)  20.2 us
    all_to_all x1, starting transfers between devices, on_device(): lax.all_to_all(up_part, FS, split_axis=1, concat_axis=0, tiled=True)  14.2 us
    all_to_all x1, waiting for transfers between devices, on_device(): lax.all_to_all(up_part, FS, split_axis=1, concat_axis=0, tiled=True)  13.8 us
    all_to_all x1, blocking collectives, on_device(): lax.all_to_all(up_cast, 'tp', split_axis=0, concat_axis=1, tiled=True)  13 us
    all_to_all x1, starting transfers between devices, copy_for_each(): lax.all_to_all(jnp.broadcast_to(array[None], (peers, *array.shape)), axis...  5.11 us
    split x3, local copies, waits for them, and re-layouts, in_one_piece(): jnp.split(whole, [sum(widths[:k]) for k in range(1, len(widths))], axis=a...  4.99 us
  transfers between devices with their start and end apart: 6, of which 5 were waited for; matrix products, arithmetic and copies ran while one was open for 2% of the time, Pallas kernels for 0%

commit v1 on v0

v1 whole, which is shorter than its diff:
```python
import jax
import jax.numpy as jnp
from jax import lax
from jax.experimental import pallas as pl
from jax.experimental.pallas import tpu as pltpu
from jax.sharding import Mesh
from jax.sharding import PartitionSpec as P

MESH = pl.DeviceIdType.MESH
AXES = ("fz", "fy", "fc", "tp")
BF16 = jnp.bfloat16
F32 = jnp.float32
FAR_FIRST = (4, 3, 5, 2, 6, 1, 7)


def remote(src, dst, send, recv, device):
    return pltpu.make_async_remote_copy(
        src_ref=src, dst_ref=dst, send_sem=send, recv_sem=recv, device_id=device, device_id_type=MESH
    )


def kernel(
    tokens_hbm, gain_ref, gate_hbm, up_hbm, down_hbm,
    gate_out, up_out, down_out, mixed_out,
    tok, gate_in, up_in, down_in, packed, r1, r2, w, normed, db, parts, got, pieces, got2, last, mix, gate_v, up_v,
    in_sem, out_sem, xs, xr, as_, ar, bs, br, ds, dr, gs, gr, cs, cr, es, er, ps, pr, qs, qr, fs, fr,
):
    z, y, c, x = (lax.axis_index(a) for a in AXES)
    right, left, opposite = lax.rem(x + 1, 4), lax.rem(x + 3, 4), lax.rem(x + 2, 4)
    partner = (z, y, 1 - c, x)

    def x_peer(p):
        return (z, y, c, p)

    first = jnp.where(c == 0, y, z)
    second = jnp.where(c == 0, z, y)

    def first_peer(p):
        return (jnp.where(c == 0, z, p), jnp.where(c == 0, p, y), c, x)

    def second_peer(p):
        return (jnp.where(c == 0, p, z), jnp.where(c == 0, y, p), c, x)

    barrier = pltpu.get_barrier_semaphore()
    peers = [x_peer(lax.rem(x + k, 4)) for k in (1, 2, 3)]
    peers += [first_peer(lax.rem(first + k, 8)) for k in range(1, 8)]
    peers += [second_peer(lax.rem(second + k, 8)) for k in range(1, 8)]
    peers += [partner]
    for peer in peers:
        pl.semaphore_signal(barrier, inc=1, device_id=peer, device_id_type=MESH)

    row = pl.multiple_of(96 * c, 32)
    loads = [
        pltpu.make_async_copy(gate_hbm, gate_in, in_sem.at[0]),
        pltpu.make_async_copy(up_hbm, up_in, in_sem.at[1]),
        pltpu.make_async_copy(down_hbm, down_in, in_sem.at[2]),
        pltpu.make_async_copy(tokens_hbm.at[pl.ds(row, 96)], tok, in_sem.at[3]),
    ]
    for load in loads:
        load.start()

    lanes = lax.broadcasted_iota(jnp.int32, (32, 32), 1)
    rows = lax.broadcasted_iota(jnp.int32, (32, 32), 0)
    spread = jnp.broadcast_to(gain_ref[...], (32, 32))
    gain = jnp.sum(jnp.where(lanes == rows, spread, 0.0), axis=1, keepdims=True)
    loads[0].wait()
    loads[1].wait()
    for s in range(4):
        scale = gain[8 * s : 8 * s + 8]
        g = gate_in[8 * s : 8 * s + 8, :] * scale
        u = up_in[8 * s : 8 * s + 8, :] * scale
        for j in range(16):
            cut = slice(176 * j, 176 * j + 176)
            unit = jnp.concatenate([g[:, cut], u[:, cut], jnp.zeros((8, 32), F32)], axis=1)
            packed[s, j // 8, j % 8] = unit.astype(BF16)

    pl.semaphore_wait(barrier, 18)

    x_sends = []
    for k in (2, 1, 3):
        p = lax.rem(x + k, 4)
        send = remote(packed.at[p], r1.at[pl.ds(2 * x, 2)], xs.at[k], xr.at[k], x_peer(p))
        send.start()
        x_sends.append(send)
    r1[pl.ds(2 * x, 2)] = packed[x]

    loads[2].wait()
    for i in range(11):
        db[c, x, i] = down_in[8 * i : 8 * i + 8, :].astype(BF16)

    def down_half(t, h):
        return db.at[c, t, :, :, pl.ds(512 * h, 512)]

    def down_copy(t, h, k, p):
        return remote(down_half(t, h), down_half(t, h), ds.at[k], dr.at[k], x_peer(p))

    d_sends = [
        down_copy(x, 0, 0, right), down_copy(x, 1, 1, left), down_copy(x, 1, 2, right), down_copy(x, 0, 3, left)
    ]
    for send in d_sends:
        send.start()

    for send in x_sends:
        send.wait_recv()

    a_sends = []
    for k in FAR_FIRST:
        p = lax.rem(first + k, 8)

        @pl.when(c == 0)
        def _():
            remote(r1.at[:, p], r2.at[first], as_.at[k], ar.at[k], first_peer(p)).start()

        @pl.when(c == 1)
        def _():
            remote(r1.at[p], r2.at[first], as_.at[k], ar.at[k], first_peer(p)).start()

        a_sends.append(remote(r1.at[p], r2.at[first], as_.at[k], ar.at[k], first_peer(p)))

    @pl.when(c == 0)
    def _():
        r2[first] = r1[:, first]

    @pl.when(c == 1)
    def _():
        r2[first] = r1[first]

    loads[3].wait()

    def norm_rows(i, carry):
        part = tok[pl.ds(pl.multiple_of(16 * i, 16), 16), :].astype(F32)
        mean = jnp.mean(part * part, axis=-1, keepdims=True)
        normed[pl.ds(pl.multiple_of(16 * i, 16), 16), :] = (part * lax.rsqrt(mean + 1e-06)).astype(BF16)
        return carry

    lax.fori_loop(0, 6, norm_rows, 0)

    for send in a_sends:
        send.wait_recv()

    b_sends = []
    for k in FAR_FIRST:
        p = lax.rem(second + k, 8)

        @pl.when(c == 0)
        def _():
            remote(r2.at[:, p], w.at[second, :, c, x], bs.at[k], br.at[k], second_peer(p)).start()

        @pl.when(c == 1)
        def _():
            remote(r2.at[:, p], w.at[:, second, c, x], bs.at[k], br.at[k], second_peer(p)).start()

        b_sends.append(remote(r2.at[:, p], w.at[second, :, c, x], bs.at[k], br.at[k], second_peer(p)))

    @pl.when(c == 0)
    def _():
        w[second, :, c, x] = r2[:, second]

    @pl.when(c == 1)
    def _():
        w[:, second, c, x] = r2[:, second]

    d_sends[0].wait_recv()
    forward = down_copy(left, 0, 4, right)
    forward.start()
    d_sends.append(forward)
    d_sends[1].wait_recv()
    forward = down_copy(right, 1, 5, left)
    forward.start()
    d_sends.append(forward)

    for send in b_sends:
        send.wait_recv()

    def block(core, s, h, g):
        return w.at[pl.ds(4 * h, 4), pl.ds(4 * g, 4), core, s]

    def gather_copy(s, h, g, k, p):
        return remote(block(c, s, h, g), block(c, s, h, g), gs.at[h, k], gr.at[h, k], x_peer(p))

    def core_copy(s, h, g, k):
        return remote(block(c, s, h, g), block(c, s, h, g), cs.at[h, k], cr.at[h, k], partner)

    g_sends = []
    c_sends = []
    acc = jnp.zeros((96, 384), F32)
    for h in range(2):
        ways = [
            gather_copy(x, h, 0, 0, right), gather_copy(x, h, 1, 1, left),
            gather_copy(x, h, 1, 2, right), gather_copy(x, h, 0, 3, left),
        ]
        for send in ways:
            send.start()
        swaps = []

        def swap(s, g, k):
            send = core_copy(s, h, g, k)
            send.start()
            swaps.append(send)

        swap(x, 0, 0)
        swap(x, 1, 1)
        ways[0].wait_recv()
        forward = gather_copy(left, h, 0, 4, right)
        forward.start()
        ways.append(forward)
        swap(left, 0, 2)
        ways[1].wait_recv()
        forward = gather_copy(right, h, 1, 5, left)
        forward.start()
        ways.append(forward)
        swap(right, 1, 3)
        ways[2].wait_recv()
        swap(left, 1, 4)
        ways[3].wait_recv()
        swap(right, 0, 5)
        g_sends.append(ways)
        c_sends.append(swaps)
        if h == 0:
            for send in d_sends[2:]:
                send.wait_recv()
            whole = remote(db.at[c], db.at[c], es, er, partner)
            whole.start()
    for h in range(2):
        for k, g in ((4, 0), (5, 1)):
            g_sends[h][k].wait_recv()
            send = core_copy(opposite, h, g, 6 + g)
            send.start()
            c_sends[h].append(send)
        for send in c_sends[h]:
            send.wait_recv()
        acc += jnp.dot(
            normed[:, 2048 * h : 2048 * h + 2048],
            w[4 * h : 4 * h + 4].reshape(2048, 384),
            preferred_element_type=F32,
        )
    gate = acc[:, :176]
    up = acc[:, 176:352]
    hidden = (gate * (1.0 / (1.0 + jnp.exp(-gate))) * up).astype(BF16)
    whole.wait_recv()

    def piece_send(p, k):
        return remote(parts.at[p], got.at[first], ps.at[k], pr.at[k], first_peer(p))

    @pl.when(c == 0)
    def _():
        for p in range(8):
            cols = [
                db[:, q // 2, :, :, 512 * (q % 2) + 64 * p : 512 * (q % 2) + 64 * p + 64].reshape(176, 64)
                for q in range(8)
            ]
            parts[p] = jnp.dot(hidden, jnp.concatenate(cols, axis=1), preferred_element_type=F32).astype(BF16)

    @pl.when(c == 1)
    def _():
        for p in range(8):
            cols = db[:, p // 2, :, :, 512 * (p % 2) : 512 * (p % 2) + 512].reshape(176, 512)
            parts[p] = jnp.dot(hidden, cols, preferred_element_type=F32).astype(BF16)

    p_sends = []
    for k in FAR_FIRST:
        send = piece_send(lax.rem(first + k, 8), k)
        send.start()
        p_sends.append(send)

    for core in range(2):
        @pl.when(c == core)
        def _():
            def unpack(i, carry):
                rows = w[i]
                gate_v[i] = rows[..., 88 * core : 88 * core + 88]
                up_v[i] = rows[..., 176 + 88 * core : 264 + 88 * core]
                return carry

            lax.fori_loop(0, 8, unpack, 0)

    outs = [
        pltpu.make_async_copy(gate_v, gate_out, out_sem.at[0]),
        pltpu.make_async_copy(up_v, up_out, out_sem.at[1]),
    ]
    for t in range(4):
        outs.append(pltpu.make_async_copy(db.at[c, t], down_out.at[:, :, pl.ds(1024 * t, 1024)], out_sem.at[2 + t]))
    for out in outs:
        out.start()

    for send in p_sends:
        send.wait_recv()
    total = parts[first].astype(F32)
    for k in FAR_FIRST:
        total += got[lax.rem(first + k, 8)].astype(F32)
    for q in range(8):
        pieces[q] = total[:, 64 * q : 64 * q + 64].astype(BF16)
    q_sends = []
    for k in FAR_FIRST:
        p = lax.rem(second + k, 8)
        send = remote(pieces.at[p], got2.at[second], qs.at[k], qr.at[k], second_peer(p))
        send.start()
        q_sends.append(send)
    for send in q_sends:
        send.wait_recv()
    total = pieces[second].astype(F32)
    for k in FAR_FIRST:
        total += got2[lax.rem(second + k, 8)].astype(F32)

    @pl.when(c == 0)
    def _():
        mix[c] = total[:, :32].astype(BF16)
        last[...] = total[:, 32:].astype(BF16)

    @pl.when(c == 1)
    def _():
        mix[c] = total[:, 32:].astype(BF16)
        last[...] = total[:, :32].astype(BF16)

    swap_last = remote(last, mix.at[c], fs, fr, partner)
    swap_last.start()
    swap_last.wait_recv()
    out = pltpu.make_async_copy(mix, mixed_out, out_sem.at[6])
    out.start()
    for send in x_sends + d_sends + a_sends + b_sends + p_sends + q_sends:
        send.wait_send()
    for ways in g_sends + c_sends:
        for send in ways:
            send.wait_send()
    whole.wait_send()
    swap_last.wait_send()
    for out_copy in outs:
        out_copy.wait()
    out.wait()


def on_device(prompt_tokens, norm_gain, gate_trained, up_trained, down_trained):
    dma = pltpu.SemaphoreType.DMA
    hbm = pl.BlockSpec(memory_space=pl.ANY)
    vmem = pltpu.VMEM
    gate, up, down, mixed = pl.pallas_call(
        kernel,
        out_shape=(
            jax.ShapeDtypeStruct((8, 8, 2, 4, 8, 88), BF16),
            jax.ShapeDtypeStruct((8, 8, 2, 4, 8, 88), BF16),
            jax.ShapeDtypeStruct((11, 8, 4096), BF16),
            jax.ShapeDtypeStruct((2, 96, 32), BF16),
        ),
        in_specs=[hbm, pl.BlockSpec(memory_space=pltpu.VMEM), hbm, hbm, hbm],
        out_specs=(hbm, hbm, hbm, hbm),
        scratch_shapes=[
            vmem((96, 4096), BF16),
            vmem((32, 2816), F32),
            vmem((32, 2816), F32),
            vmem((88, 1024), F32),
            vmem((4, 2, 8, 8, 384), BF16),
            vmem((8, 8, 8, 384), BF16),
            vmem((8, 8, 8, 384), BF16),
            vmem((8, 8, 2, 4, 8, 384), BF16),
            vmem((96, 4096), BF16),
            vmem((2, 4, 11, 8, 1024), BF16),
            vmem((8, 96, 512), BF16),
            vmem((8, 96, 512), BF16),
            vmem((8, 96, 64), BF16),
            vmem((8, 96, 64), BF16),
            vmem((96, 32), BF16),
            vmem((2, 96, 32), BF16),
            vmem((8, 8, 2, 4, 8, 88), BF16),
            vmem((8, 8, 2, 4, 8, 88), BF16),
            dma((4,)), dma((7,)),
            dma((4,)), dma((4,)),
            dma((8,)), dma((8,)),
            dma((8,)), dma((8,)),
            dma((6,)), dma((6,)),
            dma((2, 6)), dma((2, 6)),
            dma((2, 8)), dma((2, 8)),
            dma, dma,
            dma((8,)), dma((8,)),
            dma((8,)), dma((8,)),
            dma, dma,
        ],
        compiler_params=pltpu.CompilerParams(
            collective_id=0, has_side_effects=True, vmem_limit_bytes=48 * 1024 * 1024
        ),
    )(prompt_tokens, norm_gain.reshape(1, 32), gate_trained, up_trained, down_trained)
    return gate.reshape(4096, 88), up.reshape(4096, 88), down.reshape(88, 4096), mixed.reshape(192, 32)


def solution(mesh):
    finer = Mesh(mesh.devices.reshape(8, 8, 2, mesh.shape["tp"]), AXES)
    rows = AXES[:3]
    return jax.shard_map(
        on_device,
        mesh=finer,
        in_specs=(P("tp", None), P(rows), P(rows, "tp"), P(rows, "tp"), P(rows, "tp")),
        out_specs=(P(None, rows), P(None, rows), P(rows, None), P("tp", rows)),
        check_vma=False,
    )
```

time: 246 us -> 83.5 us (0.34)
  the two profiles are of different devices: /device:TPU:2 before, /device:TPU:1 now
where the time goes in v1:
time: 83.5 us; the launch traced here: 83.2 us
  Pallas kernels  73.6 us (88%)
  local copies, waits for them, and re-layouts  9.01 us (11%)
    pallas_call x1, Pallas kernels, on_device(): pl.pallas_call(kernel, out_shape=(jax.ShapeDtypeStruct((8, 8, 2, 4, 8, 88...  73.6 us
    unnamed x14, local copies, waits for them, and re-layouts  9.01 us

profile of v1, /device:TPU:1, one launch (start us, length us, event | category | flops | bytes accessed | tf_op | source)
XLA Modules:
  0.0 83.2 jit_solution(13465608860807351726)
XLA Ops:
  0.6 0.0 copy-start
  0.6 1.4 %copy-done = bf16[192,4096]{1,0:T(8,128)(2,1)S(1)} copy-done((bf16[192,4096]{1,0:T(8,128)(2,1)S(1)}, bf16[192,4096]{1,0:T(8,128)(2,1)}, u32[]{:S(2)}) %copy-start) | copy-done | bytes 1572888
  2.0 0.0 copy-start.1
  2.0 1.0 %copy-done.1 = f32[32,2816]{1,0:T(8,128)S(1)} copy-done((f32[32,2816]{1,0:T(8,128)S(1)}, f32[32,2816]{1,0:T(8,128)}, u32[]{:S(2)}) %copy-start.1) | copy-done | bytes 360472
  3.0 0.0 copy-start.2
  3.0 1.0 %copy-done.2 = f32[32,2816]{1,0:T(8,128)S(1)} copy-done((f32[32,2816]{1,0:T(8,128)S(1)}, f32[32,2816]{1,0:T(8,128)}, u32[]{:S(2)}) %copy-start.2) | copy-done | bytes 360472
  4.0 0.0 copy-start.3
  4.0 1.0 %copy-done.3 = f32[88,1024]{1,0:T(8,128)S(1)} copy-done((f32[88,1024]{1,0:T(8,128)S(1)}, f32[88,1024]{1,0:T(8,128)}, u32[]{:S(2)}) %copy-start.3) | copy-done | bytes 360472
  5.0 0.0 copy-start.4
  5.0 0.7 copy-done.4
  5.7 73.6 %shard_map.84 = (bf16[8,8,2,4,8,88]{5,4,3,2,1,0:T(8,128)(2,1)S(1)}, bf16[8,8,2,4,8,88]{5,4,3,2,1,0:T(8,128)(2,1)S(1)}, bf16[11,8,4096]{2,1,0:T(8,128)(2,1)S(1)}, bf16[2,96,32]{2,1,0:T(8,128)(2,1)S(1)}) custom-call(bf16[192,4096]{1,0:T(8,128)(2,1)S(1)} %copy-done, f32[1,32]{1,0:T(1,128)S(1)} %bitcast.9, f32[32,2816]{1,0:T(8,128)S(1)} %copy-done.1, ...), custom_call_target="tpu_custom_call" | custom-call | tf_op jit(solution)/shard_map/pallas_call | solution.py:336
  79.2 1.2 %copy.9 = bf16[4096,88]{0,1:T(8,128)(2,1)} copy(bf16[4096,88]{1,0:T(8,128)(2,1)S(1)} %bitcast.6) | data formatting | bytes 1441792
  80.5 1.2 %copy.10 = bf16[4096,88]{0,1:T(8,128)(2,1)} copy(bf16[4096,88]{1,0:T(8,128)(2,1)S(1)} %bitcast.5) | data formatting | bytes 1441792
  81.7 0.7 copy.11
  82.4 0.9 %copy.13 = bf16[88,4096]{1,0:T(8,128)(2,1)} copy(bf16[88,4096]{1,0:T(8,128)(2,1)S(1)} %bitcast.7) | data formatting | bytes 1441792
Async XLA Ops:
  0.6 1.4 %copy-start = (bf16[192,4096]{1,0:T(8,128)(2,1)S(1)}, bf16[192,4096]{1,0:T(8,128)(2,1)}, u32[]{:S(2)}) copy-start(bf16[192,4096]{1,0:T(8,128)(2,1)} %tokens_hbm.1) | copy-start | bytes 4718596
  2.0 1.0 %copy-start.1 = (f32[32,2816]{1,0:T(8,128)S(1)}, f32[32,2816]{1,0:T(8,128)}, u32[]{:S(2)}) copy-start(f32[32,2816]{1,0:T(8,128)} %gate_hbm.1) | copy-start | bytes 1081348
  3.0 1.0 %copy-start.2 = (f32[32,2816]{1,0:T(8,128)S(1)}, f32[32,2816]{1,0:T(8,128)}, u32[]{:S(2)}) copy-start(f32[32,2816]{1,0:T(8,128)} %up_hbm.1) | copy-start | bytes 1081348
  4.0 1.0 %copy-start.3 = (f32[88,1024]{1,0:T(8,128)S(1)}, f32[88,1024]{1,0:T(8,128)}, u32[]{:S(2)}) copy-start(f32[88,1024]{1,0:T(8,128)} %down_hbm.1) | copy-start | bytes 1081348
  5.0 0.7 copy-start.4

commit v2 on v1

v2 whole, which is shorter than its diff:
```python
import jax
import jax.numpy as jnp
from jax import lax
from jax.experimental import pallas as pl
from jax.experimental.pallas import tpu as pltpu
from jax.sharding import Mesh
from jax.sharding import PartitionSpec as P

MESH = pl.DeviceIdType.MESH
AXES = ("fz", "fy", "fc", "tp")
BF16 = jnp.bfloat16
F32 = jnp.float32
LIMIT = 40 * 1024 * 1024
FAR_FIRST = (4, 3, 5, 2, 6, 1, 7)


def remote(src, dst, send, recv, device):
    return pltpu.make_async_remote_copy(
        src_ref=src, dst_ref=dst, send_sem=send, recv_sem=recv, device_id=device, device_id_type=MESH
    )


class Flights:
    def __init__(self):
        self.all = []
        self.landed = set()

    def note(self, copy):
        self.all.append(copy)
        return copy

    def go(self, copy):
        copy.start()
        return self.note(copy)

    def land(self, copy):
        copy.wait_recv()
        self.landed.add(id(copy))

    def finish(self):
        for copy in self.all:
            if id(copy) not in self.landed:
                copy.wait_recv()
        for copy in self.all:
            copy.wait_send()


def kernel(
    tokens_hbm, gain_hbm, gate_hbm, up_hbm, down_hbm,
    gate_out, up_out, down_out, mixed_out,
    tok, gain_in, gate_in, up_in, down_in, packed, r1, r2, w, normed, db, parts, got, pieces, got2, last, mix,
    in_sem, xs, xr, as_, ar, bs, br, ds, dr, gs, gr, cs, cr, es, er, ps, pr, qs, qr, fs, fr,
):
    z, y, c, x = (lax.axis_index(a) for a in AXES)
    right, left, opposite = lax.rem(x + 1, 4), lax.rem(x + 3, 4), lax.rem(x + 2, 4)
    partner = (z, y, 1 - c, x)
    flights = Flights()
    go, land = flights.go, flights.land

    def x_peer(p):
        return (z, y, c, p)

    first = jnp.where(c == 0, y, z)
    second = jnp.where(c == 0, z, y)

    def first_peer(p):
        return (jnp.where(c == 0, z, p), jnp.where(c == 0, p, y), c, x)

    def second_peer(p):
        return (jnp.where(c == 0, p, z), jnp.where(c == 0, y, p), c, x)

    barrier = pltpu.get_barrier_semaphore()
    peers = [x_peer(lax.rem(x + k, 4)) for k in (1, 2, 3)]
    peers += [first_peer(lax.rem(first + k, 8)) for k in range(1, 8)]
    peers += [second_peer(lax.rem(second + k, 8)) for k in range(1, 8)]
    peers += [partner]
    row = pl.multiple_of(96 * c, 32)
    loads = [
        pltpu.make_async_copy(gate_hbm, gate_in, in_sem.at[0]),
        pltpu.make_async_copy(up_hbm, up_in, in_sem.at[1]),
        pltpu.make_async_copy(down_hbm, down_in, in_sem.at[2]),
        pltpu.make_async_copy(tokens_hbm.at[pl.ds(row, 96)], tok, in_sem.at[3]),
        pltpu.make_async_copy(gain_hbm, gain_in, in_sem.at[4]),
    ]
    for load in loads:
        load.start()
    for peer in peers:
        pl.semaphore_signal(barrier, inc=1, device_id=peer, device_id_type=MESH)

    lanes = lax.broadcasted_iota(jnp.int32, (32, 32), 1)
    rows = lax.broadcasted_iota(jnp.int32, (32, 32), 0)
    loads[4].wait()
    spread = jnp.broadcast_to(gain_in[...], (32, 32))
    gain = jnp.sum(jnp.where(lanes == rows, spread, 0.0), axis=1, keepdims=True)
    loads[0].wait()
    loads[1].wait()
    for s in range(4):
        scale = gain[8 * s : 8 * s + 8]
        g = gate_in[8 * s : 8 * s + 8, :] * scale
        u = up_in[8 * s : 8 * s + 8, :] * scale
        for j in range(16):
            cut = slice(176 * j, 176 * j + 176)
            unit = jnp.concatenate([g[:, cut], u[:, cut], jnp.zeros((8, 32), F32)], axis=1).astype(BF16)
            for n in range(3):
                packed[n, s, j // 8, j % 8] = unit[:, 128 * n : 128 * n + 128]

    pl.semaphore_wait(barrier, 18)
    x_sends = []
    for n in range(3):
        x_sends.append([])
        for k in (2, 1, 3):
            p = lax.rem(x + k, 4)
            x_sends[n].append(
                go(remote(packed.at[n, p], r1.at[n, pl.ds(2 * x, 2)], xs.at[n, k], xr.at[n, k], x_peer(p)))
            )

    loads[2].wait()
    for i in range(11):
        db[c, x, i] = down_in[8 * i : 8 * i + 8, :].astype(BF16)

    def down_copy(t, h, k, p):
        half = db.at[c, t, :, :, pl.ds(512 * h, 512)]
        return remote(half, half, ds.at[k], dr.at[k], x_peer(p))

    d_ways = [
        go(down_copy(x, 0, 0, right)), go(down_copy(x, 1, 1, left)),
        go(down_copy(x, 1, 2, right)), go(down_copy(x, 0, 3, left)),
    ]

    for n in range(3):
        r1[n, pl.ds(2 * x, 2)] = packed[n, x]

    a_sends = []
    for n in range(3):
        for send in x_sends[n]:
            land(send)
        a_sends.append([])
        for k in FAR_FIRST:
            p = lax.rem(first + k, 8)
            sems = as_.at[n, k], ar.at[n, k]

            @pl.when(c == 0)
            def _():
                remote(r1.at[n, :, p], r2.at[n, first], *sems, first_peer(p)).start()

            @pl.when(c == 1)
            def _():
                remote(r1.at[n, p], r2.at[n, first], *sems, first_peer(p)).start()

            a_sends[n].append(flights.note(remote(r1.at[n, p], r2.at[n, first], *sems, first_peer(p))))

        @pl.when(c == 0)
        def _():
            r2[n, first] = r1[n, :, first]

        @pl.when(c == 1)
        def _():
            r2[n, first] = r1[n, first]

    loads[3].wait()

    def norm_rows(i, carry):
        part = tok[pl.ds(pl.multiple_of(16 * i, 16), 16), :].astype(F32)
        mean = jnp.mean(part * part, axis=-1, keepdims=True)
        normed[pl.ds(pl.multiple_of(16 * i, 16), 16), :] = (part * lax.rsqrt(mean + 1e-06)).astype(BF16)
        return carry

    lax.fori_loop(0, 6, norm_rows, 0)

    b_sends = []
    for n in range(3):
        for send in a_sends[n]:
            land(send)
        b_sends.append([])
        for k in FAR_FIRST:
            p = lax.rem(second + k, 8)
            sems = bs.at[n, k], br.at[n, k]

            @pl.when(c == 0)
            def _():
                remote(r2.at[n, :, p], w.at[n, second, :, c, x], *sems, second_peer(p)).start()

            @pl.when(c == 1)
            def _():
                remote(r2.at[n, :, p], w.at[n, :, second, c, x], *sems, second_peer(p)).start()

            b_sends[n].append(
                flights.note(remote(r2.at[n, :, p], w.at[n, second, :, c, x], *sems, second_peer(p)))
            )

        @pl.when(c == 0)
        def _():
            w[n, second, :, c, x] = r2[n, :, second]

        @pl.when(c == 1)
        def _():
            w[n, :, second, c, x] = r2[n, :, second]

        if n == 0:
            land(d_ways[0])
            d_ways.append(go(down_copy(left, 0, 4, right)))
            land(d_ways[1])
            d_ways.append(go(down_copy(right, 1, 5, left)))

    def gather_copy(s, n, h, k, p):
        half = w.at[n, :, pl.ds(4 * h, 4), c, s]
        return remote(half, half, gs.at[n, k], gr.at[n, k], x_peer(p))

    def core_copy(s, n, k):
        return remote(w.at[n, :, :, c, s], w.at[n, :, :, c, s], cs.at[n, k], cr.at[n, k], partner)

    ways = []
    swaps = []
    for n in range(3):
        for send in b_sends[n]:
            land(send)
        ways.append([
            go(gather_copy(x, n, 0, 0, right)), go(gather_copy(x, n, 1, 1, left)),
            go(gather_copy(x, n, 1, 2, right)), go(gather_copy(x, n, 0, 3, left)),
        ])
        swaps.append([go(core_copy(x, n, 0))])
    for send in d_ways[2:]:
        land(send)
    whole = go(remote(db.at[c], db.at[c], es, er, partner))
    for n in range(3):
        land(ways[n][0])
        ways[n].append(go(gather_copy(left, n, 0, 4, right)))
        land(ways[n][1])
        ways[n].append(go(gather_copy(right, n, 1, 5, left)))
        land(ways[n][2])
        swaps[n].append(go(core_copy(left, n, 1)))
        land(ways[n][3])
        swaps[n].append(go(core_copy(right, n, 2)))
    acc = []
    for n in range(3):
        land(ways[n][4])
        land(ways[n][5])
        swaps[n].append(go(core_copy(opposite, n, 3)))
        for send in swaps[n]:
            land(send)
        acc.append(jnp.dot(normed[...], w[n].reshape(4096, 128), preferred_element_type=F32))
    gate = jnp.concatenate([acc[0], acc[1][:, :48]], axis=1)
    up = jnp.concatenate([acc[1][:, 48:], acc[2][:, :96]], axis=1)
    hidden = (gate * (1.0 / (1.0 + jnp.exp(-gate))) * up).astype(BF16)
    land(whole)

    @pl.when(c == 0)
    def _():
        for p in range(8):
            cols = [
                db[:, q // 2, :, :, 512 * (q % 2) + 64 * p : 512 * (q % 2) + 64 * p + 64].reshape(176, 64)
                for q in range(8)
            ]
            parts[p] = jnp.dot(hidden, jnp.concatenate(cols, axis=1), preferred_element_type=F32).astype(BF16)

    @pl.when(c == 1)
    def _():
        for p in range(8):
            cols = db[:, p // 2, :, :, 512 * (p % 2) : 512 * (p % 2) + 512].reshape(176, 512)
            parts[p] = jnp.dot(hidden, cols, preferred_element_type=F32).astype(BF16)

    p_sends = []
    for k in FAR_FIRST:
        p = lax.rem(first + k, 8)
        p_sends.append(go(remote(parts.at[p], got.at[first], ps.at[k], pr.at[k], first_peer(p))))

    for core in range(2):
        @pl.when(c == core)
        def _():
            def unpack(i, carry):
                at = pl.ds(pl.multiple_of(512 * i, 512), 512)
                tiles = [w[n, i].reshape(512, 128).T for n in range(3)]
                for out, start in ((gate_out, 88 * core), (up_out, 176 + 88 * core)):
                    for r in range(11):
                        n, k = divmod(start + 8 * r, 128)
                        out[r, :, at] = tiles[n][k : k + 8]
                return carry

            lax.fori_loop(0, 8, unpack, 0)
    for t in range(4):
        down_out[:, :, 1024 * t : 1024 * t + 1024] = db[c, t]

    for send in p_sends:
        land(send)
    total = parts[first].astype(F32)
    for k in FAR_FIRST:
        total += got[lax.rem(first + k, 8)].astype(F32)
    for q in range(8):
        both = jnp.concatenate([total[:48, 64 * q : 64 * q + 64], total[48:, 64 * q : 64 * q + 64]], axis=1)
        pieces[q] = both.astype(BF16)
    q_sends = []
    for k in FAR_FIRST:
        p = lax.rem(second + k, 8)
        q_sends.append(go(remote(pieces.at[p], got2.at[second], qs.at[k], qr.at[k], second_peer(p))))
    for send in q_sends:
        land(send)
    total = pieces[second].astype(F32)
    for k in FAR_FIRST:
        total += got2[lax.rem(second + k, 8)].astype(F32)
    total = jnp.concatenate([total[:, :64], total[:, 64:]], axis=0)

    @pl.when(c == 0)
    def _():
        mix[c] = total[:, :32].astype(BF16)
        last[...] = total[:, 32:].astype(BF16)

    @pl.when(c == 1)
    def _():
        mix[c] = total[:, 32:].astype(BF16)
        last[...] = total[:, :32].astype(BF16)

    land(go(remote(last, mix.at[c], fs, fr, partner)))
    mixed_out[...] = jnp.concatenate([mix[0], mix[1]], axis=0).astype(F32).T.astype(BF16)
    flights.finish()


def write_out(*refs):
    sem = refs[-1]
    copies = [pltpu.make_async_copy(refs[k], refs[k + 4], sem.at[k]) for k in range(4)]
    for copy in copies:
        copy.start()
    for copy in copies:
        copy.wait()


def on_device(prompt_tokens, norm_gain, gate_trained, up_trained, down_trained):
    dma = pltpu.SemaphoreType.DMA
    hbm = pl.BlockSpec(memory_space=pltpu.HBM)
    in_vmem = pl.BlockSpec(memory_space=pltpu.VMEM)
    vmem = pltpu.VMEM
    shapes = (
        jax.ShapeDtypeStruct((11, 8, 4096), BF16),
        jax.ShapeDtypeStruct((11, 8, 4096), BF16),
        jax.ShapeDtypeStruct((11, 8, 4096), BF16),
        jax.ShapeDtypeStruct((32, 192), BF16),
    )
    results = pl.pallas_call(
        kernel,
        out_shape=[pltpu.VMEM(a.shape, a.dtype) for a in shapes],
        in_specs=[hbm] * 5,
        out_specs=(in_vmem,) * 4,
        scratch_shapes=[
            vmem((96, 4096), BF16),
            vmem((1, 32), F32),
            vmem((32, 2816), F32),
            vmem((32, 2816), F32),
            vmem((88, 1024), F32),
            vmem((3, 4, 2, 8, 8, 128), BF16),
            vmem((3, 8, 8, 8, 128), BF16),
            vmem((3, 8, 8, 8, 128), BF16),
            vmem((3, 8, 8, 2, 4, 8, 128), BF16),
            vmem((96, 4096), BF16),
            vmem((2, 4, 11, 8, 1024), BF16),
            vmem((8, 96, 512), BF16),
            vmem((8, 96, 512), BF16),
            vmem((8, 48, 128), BF16),
            vmem((8, 48, 128), BF16),
            vmem((96, 32), BF16),
            vmem((2, 96, 32), BF16),
            dma((5,)),
            dma((3, 4)), dma((3, 4)),
            dma((3, 8)), dma((3, 8)),
            dma((3, 8)), dma((3, 8)),
            dma((6,)), dma((6,)),
            dma((3, 6)), dma((3, 6)),
            dma((3, 4)), dma((3, 4)),
            dma, dma,
            dma((8,)), dma((8,)),
            dma((8,)), dma((8,)),
            dma, dma,
        ],
        compiler_params=pltpu.CompilerParams(
            collective_id=0, has_side_effects=True, vmem_limit_bytes=LIMIT
        ),
    )(
        pltpu.with_memory_space_constraint(prompt_tokens, pltpu.HBM),
        pltpu.with_memory_space_constraint(norm_gain.reshape(1, 32), pltpu.HBM),
        pltpu.with_memory_space_constraint(gate_trained, pltpu.HBM),
        pltpu.with_memory_space_constraint(up_trained, pltpu.HBM),
        pltpu.with_memory_space_constraint(down_trained, pltpu.HBM),
    )
    gate, up, down, mixed = pl.pallas_call(
        write_out,
        out_shape=shapes,
        in_specs=[in_vmem] * 4,
        out_specs=(hbm,) * 4,
        scratch_shapes=[dma((4,))],
        compiler_params=pltpu.CompilerParams(vmem_limit_bytes=1024 * 1024),
    )(*results)
    return gate.reshape(88, 4096).T, up.reshape(88, 4096).T, down.reshape(88, 4096), mixed.T


def solution(mesh):
    finer = Mesh(mesh.devices.reshape(8, 8, 2, mesh.shape["tp"]), AXES)
    rows = AXES[:3]
    return jax.shard_map(
        on_device,
        mesh=finer,
        in_specs=(P("tp", None), P(rows), P(rows, "tp"), P(rows, "tp"), P(rows, "tp")),
        out_specs=(P(None, rows), P(None, rows), P(rows, None), P("tp", rows)),
        check_vma=False,
    )
```

time: 83.5 us -> 68.7 us (0.82)
  local copies, waits for them, and re-layouts: 9.01 us -> 0 us
  Pallas kernels: 73.6 us -> 68 us
    unnamed x14 -> x0, local copies, waits for them, and re-layouts: 9.01 us -> none
    pallas_call x1 -> x2, Pallas kernels: 73.6 us -> 68 us  [the longest x1 66.6 us: on_device(): pl.pallas_call(kernel, out_shape=[pltpu.VMEM(a.shape, a.dtype) for a in s...]
where the time goes in v2:
time: 68.7 us; the launch traced here: 68.6 us
  Pallas kernels  68 us (99%)
    pallas_call x1, Pallas kernels, on_device(): pl.pallas_call(kernel, out_shape=[pltpu.VMEM(a.shape, a.dtype) for a in s...  66.6 us

profile of v2, /device:TPU:1, one launch (start us, length us, event | category | flops | bytes accessed | tf_op | source)
XLA Modules:
  0.0 68.6 jit_solution(391298845458909205)
XLA Ops:
  0.6 66.6 %shard_map.84 = (bf16[11,8,4096]{2,1,0:T(8,128)(2,1)S(1)}, bf16[11,8,4096]{2,1,0:T(8,128)(2,1)S(1)}, bf16[11,8,4096]{2,1,0:T(8,128)(2,1)S(1)}, bf16[32,192]{1,0:T(8,128)(2,1)S(1)}) custom-call(bf16[192,4096]{1,0:T(8,128)(2,1)} %tokens_hbm.1, f32[1,32]{1,0:T(1,128)} %bitcast.9, f32[32,2816]{1,0:T(8,128)} %gate_hbm.1, f32[32,2816]{1,0:T(8,128)} %up_hbm.1, ...), custom_call_target="tpu_custom_call" | custom-call | tf_op jit(solution)/shard_map/pallas_call | solution.py:337
  67.2 1.4 %shard_map.85 = (bf16[11,8,4096]{2,1,0:T(8,128)(2,1)}, bf16[11,8,4096]{2,1,0:T(8,128)(2,1)}, bf16[11,8,4096]{2,1,0:T(8,128)(2,1)}, bf16[32,192]{1,0:T(8,128)(2,1)}) custom-call(bf16[11,8,4096]{2,1,0:T(8,128)(2,1)S(1)} %get-tuple-element.12.refs_0_, bf16[11,8,4096]{2,1,0:T(8,128)(2,1)S(1)} %get-tuple-element.13.refs_1_, ...), custom_call_target="tpu_custom_call" | custom-call | tf_op jit(solution)/shard_map/pallas_call | solution.py:382

commit v3 on v2

--- a/solution.py
+++ b/solution.py
@@ -48,8 +48,8 @@
 def kernel(
     tokens_hbm, gain_hbm, gate_hbm, up_hbm, down_hbm,
     gate_out, up_out, down_out, mixed_out,
-    tok, gain_in, gate_in, up_in, down_in, packed, r1, r2, w, normed, db, parts, got, pieces, got2, last, mix,
-    in_sem, xs, xr, as_, ar, bs, br, ds, dr, gs, gr, cs, cr, es, er, ps, pr, qs, qr, fs, fr,
+    tok, gain_in, gate_in, up_in, down_in, packed, r1, r2, w, normed, tok_send, tok_all, acc, core_send, core_got, plane_send, plane_got, db, parts, got, pieces, got2, last, mix,
+    in_sem, ts, tr, us, ur, vs, vr, xs, xr, as_, ar, bs, br, ds, dr, gs, gr, cs, cr, es, er, ps, pr, qs, qr, fs, fr,
 ):
     z, y, c, x = (lax.axis_index(a) for a in AXES)
     right, left, opposite = lax.rem(x + 1, 4), lax.rem(x + 3, 4), lax.rem(x + 2, 4)
@@ -74,12 +74,11 @@
     peers += [first_peer(lax.rem(first + k, 8)) for k in range(1, 8)]
     peers += [second_peer(lax.rem(second + k, 8)) for k in range(1, 8)]
     peers += [partner]
-    row = pl.multiple_of(96 * c, 32)
     loads = [
         pltpu.make_async_copy(gate_hbm, gate_in, in_sem.at[0]),
         pltpu.make_async_copy(up_hbm, up_in, in_sem.at[1]),
         pltpu.make_async_copy(down_hbm, down_in, in_sem.at[2]),
-        pltpu.make_async_copy(tokens_hbm.at[pl.ds(row, 96)], tok, in_sem.at[3]),
+        pltpu.make_async_copy(tokens_hbm, tok, in_sem.at[3]),
         pltpu.make_async_copy(gain_hbm, gain_in, in_sem.at[4]),
     ]
     for load in loads:
@@ -114,6 +113,33 @@
                 go(remote(packed.at[n, p], r1.at[n, pl.ds(2 * x, 2)], xs.at[n, k], xr.at[n, k], x_peer(p)))
             )
 
+    loads[3].wait()
+
+    def norm_rows(i, carry):
+        part = tok[pl.ds(pl.multiple_of(16 * i, 16), 16), :].astype(F32)
+        mean = jnp.mean(part * part, axis=-1, keepdims=True)
+        normed[pl.ds(pl.multiple_of(16 * i, 16), 16), :] = (part * lax.rsqrt(mean + 1e-06)).astype(BF16)
+        return carry
+
+    lax.fori_loop(0, 12, norm_rows, 0)
+    at = lax.broadcasted_iota(jnp.int32, (512, 256), 0)
+    to = lax.broadcasted_iota(jnp.int32, (512, 256), 1)
+    source = 64 * (to % 64 // 8) + 32 * c + 8 * (to // 64) + to % 8
+    pick = jnp.where(at == source, 1.0, 0.0).astype(BF16)
+    for q in range(4):
+        even, odd = (
+            jnp.dot(normed[:, 512 * v : 512 * v + 512], pick, preferred_element_type=F32).astype(BF16)
+            for v in (2 * q, 2 * q + 1)
+        )
+        for s in range(4):
+            cut = slice(64 * s, 64 * s + 64)
+            tok_send[s, :, 128 * q : 128 * q + 128] = jnp.concatenate([even[:, cut], odd[:, cut]], axis=1)
+    t_sends = []
+    for k in (2, 1, 3):
+        p = lax.rem(x + k, 4)
+        t_sends.append(go(remote(tok_send.at[p], tok_all.at[x], ts.at[k], tr.at[k], x_peer(p))))
+    tok_all[x] = tok_send[x]
+
     loads[2].wait()
     for i in range(11):
         db[c, x, i] = down_in[8 * i : 8 * i + 8, :].astype(BF16)
@@ -157,16 +183,6 @@
         def _():
             r2[n, first] = r1[n, first]
 
-    loads[3].wait()
-
-    def norm_rows(i, carry):
-        part = tok[pl.ds(pl.multiple_of(16 * i, 16), 16), :].astype(F32)
-        mean = jnp.mean(part * part, axis=-1, keepdims=True)
-        normed[pl.ds(pl.multiple_of(16 * i, 16), 16), :] = (part * lax.rsqrt(mean + 1e-06)).astype(BF16)
-        return carry
-
-    lax.fori_loop(0, 6, norm_rows, 0)
-
     b_sends = []
     for n in range(3):
         for send in a_sends[n]:
@@ -196,32 +212,94 @@
         def _():
             w[n, :, second, c, x] = r2[n, :, second]
 
+    def gather_copy(s, n, h, k, p):
+        half = w.at[n, :, pl.ds(4 * h, 4), c, s]
+        return remote(half, half, gs.at[n, k], gr.at[n, k], x_peer(p))
+
+    def core_copy(s, n, k):
+        return remote(w.at[n, :, :, c, s], w.at[n, :, :, c, s], cs.at[n, k], cr.at[n, k], partner)
+
+    for send in t_sends:
+        land(send)
+    u_sends = []
+    for n in range(3):
+        for send in b_sends[n]:
+            land(send)
+        part = jnp.dot(
+            tok_all[...].reshape(768, 512), w[n, :, :, c, x].reshape(512, 128), preferred_element_type=F32
+        ).reshape(4, 2, 96, 128)
+        acc[n] = part
+
+        @pl.when(c == 0)
+        def _():
+            core_send[n] = part[:, 1].astype(BF16)
+
+        @pl.when(c == 1)
+        def _():
+            core_send[n] = part[:, 0].astype(BF16)
+
+        u_sends.append(go(remote(core_send.at[n], core_got.at[n], us.at[n], ur.at[n], partner)))
         if n == 0:
             land(d_ways[0])
             d_ways.append(go(down_copy(left, 0, 4, right)))
             land(d_ways[1])
             d_ways.append(go(down_copy(right, 1, 5, left)))
-
-    def gather_copy(s, n, h, k, p):
-        half = w.at[n, :, pl.ds(4 * h, 4), c, s]
-        return remote(half, half, gs.at[n, k], gr.at[n, k], x_peer(p))
-
-    def core_copy(s, n, k):
-        return remote(w.at[n, :, :, c, s], w.at[n, :, :, c, s], cs.at[n, k], cr.at[n, k], partner)
-
+    v_sends = []
+    for n in range(3):
+        land(u_sends[n])
+        plane_send[n] = (acc[n, :, c] + core_got[n].astype(F32)).astype(BF16)
+        v_sends.append([])
+        for k in (2, 1, 3):
+            p = lax.rem(x + k, 4)
+            v_sends[n].append(
+                go(remote(plane_send.at[n, p], plane_got.at[n, x], vs.at[n, k], vr.at[n, k], x_peer(p)))
+            )
+    for send in d_ways[2:]:
+        land(send)
+    whole = go(remote(db.at[c], db.at[c], es, er, partner))
     ways = []
     swaps = []
     for n in range(3):
-        for send in b_sends[n]:
-            land(send)
         ways.append([
             go(gather_copy(x, n, 0, 0, right)), go(gather_copy(x, n, 1, 1, left)),
             go(gather_copy(x, n, 1, 2, right)), go(gather_copy(x, n, 0, 3, left)),
         ])
         swaps.append([go(core_copy(x, n, 0))])
-    for send in d_ways[2:]:
-        land(send)
-    whole = go(remote(db.at[c], db.at[c], es, er, partner))
+    sums = []
+    for n in range(3):
+        for send in v_sends[n]:
+            land(send)
+        total = acc[n, x, c] + core_got[n, x].astype(F32)
+        for k in (1, 2, 3):
+            total += plane_got[n, lax.rem(x + k, 4)].astype(F32)
+        sums.append(total)
+    gate = jnp.concatenate([sums[0], sums[1][:, :48]], axis=1)
+    up = jnp.concatenate([sums[1][:, 48:], sums[2][:, :96]], axis=1)
+    hidden = (gate * (1.0 / (1.0 + jnp.exp(-gate))) * up).astype(BF16)
+    land(whole)
+
+    @pl.when(c == 0)
+    def _():
+        for p in range(8):
+            cols = [
+                db[:, q // 2, :, :, 512 * (q % 2) + 64 * p : 512 * (q % 2) + 64 * p + 64].reshape(176, 64)
+                for q in range(8)
+            ]
+            parts[p] = jnp.dot(hidden, jnp.concatenate(cols, axis=1), preferred_element_type=F32).astype(BF16)
+
+    @pl.when(c == 1)
+    def _():
+        for p in range(8):
+            cols = db[:, p // 2, :, :, 512 * (p % 2) : 512 * (p % 2) + 512].reshape(176, 512)
+            parts[p] = jnp.dot(hidden, cols, preferred_element_type=F32).astype(BF16)
+
+    p_sends = []
+    for k in FAR_FIRST:
+        p = lax.rem(first + k, 8)
+        p_sends.append(go(remote(parts.at[p], got.at[first], ps.at[k], pr.at[k], first_peer(p))))
+
+    for t in range(4):
+        down_out[:, :, 1024 * t : 1024 * t + 1024] = db[c, t]
     for n in range(3):
         land(ways[n][0])
         ways[n].append(go(gather_copy(left, n, 0, 4, right)))
@@ -231,54 +309,6 @@
         swaps[n].append(go(core_copy(left, n, 1)))
         land(ways[n][3])
         swaps[n].append(go(core_copy(right, n, 2)))
-    acc = []
-    for n in range(3):
-        land(ways[n][4])
-        land(ways[n][5])
-        swaps[n].append(go(core_copy(opposite, n, 3)))
-        for send in swaps[n]:
-            land(send)
-        acc.append(jnp.dot(normed[...], w[n].reshape(4096, 128), preferred_element_type=F32))
-    gate = jnp.concatenate([acc[0], acc[1][:, :48]], axis=1)
-    up = jnp.concatenate([acc[1][:, 48:], acc[2][:, :96]], axis=1)
-    hidden = (gate * (1.0 / (1.0 + jnp.exp(-gate))) * up).astype(BF16)
-    land(whole)
-
-    @pl.when(c == 0)
-    def _():
-        for p in range(8):
-            cols = [
-                db[:, q // 2, :, :, 512 * (q % 2) + 64 * p : 512 * (q % 2) + 64 * p + 64].reshape(176, 64)
-                for q in range(8)
-            ]
-            parts[p] = jnp.dot(hidden, jnp.concatenate(cols, axis=1), preferred_element_type=F32).astype(BF16)
-
-    @pl.when(c == 1)
-    def _():
-        for p in range(8):
-            cols = db[:, p // 2, :, :, 512 * (p % 2) : 512 * (p % 2) + 512].reshape(176, 512)
-            parts[p] = jnp.dot(hidden, cols, preferred_element_type=F32).astype(BF16)
-
-    p_sends = []
-    for k in FAR_FIRST:
-        p = lax.rem(first + k, 8)
-        p_sends.append(go(remote(parts.at[p], got.at[first], ps.at[k], pr.at[k], first_peer(p))))
-
-    for core in range(2):
-        @pl.when(c == core)
-        def _():
-            def unpack(i, carry):
-                at = pl.ds(pl.multiple_of(512 * i, 512), 512)
-                tiles = [w[n, i].reshape(512, 128).T for n in range(3)]
-                for out, start in ((gate_out, 88 * core), (up_out, 176 + 88 * core)):
-                    for r in range(11):
-                        n, k = divmod(start + 8 * r, 128)
-                        out[r, :, at] = tiles[n][k : k + 8]
-                return carry
-
-            lax.fori_loop(0, 8, unpack, 0)
-    for t in range(4):
-        down_out[:, :, 1024 * t : 1024 * t + 1024] = db[c, t]
 
     for send in p_sends:
         land(send)
@@ -292,6 +322,27 @@
     for k in FAR_FIRST:
         p = lax.rem(second + k, 8)
         q_sends.append(go(remote(pieces.at[p], got2.at[second], qs.at[k], qr.at[k], second_peer(p))))
+    for n in range(3):
+        land(ways[n][4])
+        land(ways[n][5])
+        swaps[n].append(go(core_copy(opposite, n, 3)))
+    for n in range(3):
+        for send in swaps[n]:
+            land(send)
+        for core in range(2):
+            @pl.when(c == core)
+            def _():
+                def unpack(i, carry):
+                    at = pl.ds(pl.multiple_of(512 * i, 512), 512)
+                    tile = w[n, i].reshape(512, 128).T
+                    for out, start in ((gate_out, 88 * core), (up_out, 176 + 88 * core)):
+                        for r in range(11):
+                            k = start + 8 * r - 128 * n
+                            if 0 <= k < 128:
+                                out[r, :, at] = tile[k : k + 8]
+                    return carry
+
+                lax.fori_loop(0, 8, unpack, 0)
     for send in q_sends:
         land(send)
     total = pieces[second].astype(F32)
@@ -340,7 +391,7 @@
         in_specs=[hbm] * 5,
         out_specs=(in_vmem,) * 4,
         scratch_shapes=[
-            vmem((96, 4096), BF16),
+            vmem((192, 4096), BF16),
             vmem((1, 32), F32),
             vmem((32, 2816), F32),
             vmem((32, 2816), F32),
@@ -349,7 +400,14 @@
             vmem((3, 8, 8, 8, 128), BF16),
             vmem((3, 8, 8, 8, 128), BF16),
             vmem((3, 8, 8, 2, 4, 8, 128), BF16),
-            vmem((96, 4096), BF16),
+            vmem((192, 4096), BF16),
+            vmem((4, 192, 512), BF16),
+            vmem((4, 192, 512), BF16),
+            vmem((3, 4, 2, 96, 128), F32),
+            vmem((3, 4, 96, 128), BF16),
+            vmem((3, 4, 96, 128), BF16),
+            vmem((3, 4, 96, 128), BF16),
+            vmem((3, 4, 96, 128), BF16),
             vmem((2, 4, 11, 8, 1024), BF16),
             vmem((8, 96, 512), BF16),
             vmem((8, 96, 512), BF16),
@@ -358,6 +416,9 @@
             vmem((96, 32), BF16),
             vmem((2, 96, 32), BF16),
             dma((5,)),
+            dma((4,)), dma((4,)),
+            dma((3,)), dma((3,)),
+            dma((3, 4)), dma((3, 4)),
             dma((3, 4)), dma((3, 4)),
             dma((3, 8)), dma((3, 8)),
             dma((3, 8)), dma((3, 8)),

time: 68.7 us -> 64.9 us (0.945)
  Pallas kernels: 68 us -> 64.1 us
    pallas_call x1, Pallas kernels: 66.6 us -> 62.7 us  [on_device(): pl.pallas_call(kernel, out_shape=[pltpu.VMEM(a.shape, a.dtype) for a in s...]
where the time goes in v3:
time: 64.9 us; the launch traced here: 64.7 us
  Pallas kernels  64.1 us (99%)
    pallas_call x1, Pallas kernels, on_device(): pl.pallas_call(kernel, out_shape=[pltpu.VMEM(a.shape, a.dtype) for a in s...  62.7 us
    pallas_call x1, Pallas kernels, on_device(): pl.pallas_call(write_out, out_shape=shapes, in_specs=[in_vmem] * 4, out_s...  1.37 us

profile of v3, /device:TPU:1, one launch (start us, length us, event | category | flops | bytes accessed | tf_op | source)
XLA Modules:
  0.0 64.7 jit_solution(14530339703097333175)
XLA Ops:
  0.6 62.7 %shard_map.84 = (bf16[11,8,4096]{2,1,0:T(8,128)(2,1)S(1)}, bf16[11,8,4096]{2,1,0:T(8,128)(2,1)S(1)}, bf16[11,8,4096]{2,1,0:T(8,128)(2,1)S(1)}, bf16[32,192]{1,0:T(8,128)(2,1)S(1)}) custom-call(bf16[192,4096]{1,0:T(8,128)(2,1)} %tokens_hbm.1, f32[1,32]{1,0:T(1,128)} %bitcast.9, f32[32,2816]{1,0:T(8,128)} %gate_hbm.1, f32[32,2816]{1,0:T(8,128)} %up_hbm.1, ...), custom_call_target="tpu_custom_call" | custom-call | tf_op jit(solution)/shard_map/pallas_call | solution.py:388
  63.4 1.4 %shard_map.85 = (bf16[11,8,4096]{2,1,0:T(8,128)(2,1)}, bf16[11,8,4096]{2,1,0:T(8,128)(2,1)}, bf16[11,8,4096]{2,1,0:T(8,128)(2,1)}, bf16[32,192]{1,0:T(8,128)(2,1)}) custom-call(bf16[11,8,4096]{2,1,0:T(8,128)(2,1)S(1)} %get-tuple-element.12.refs_0_, bf16[11,8,4096]{2,1,0:T(8,128)(2,1)S(1)} %get-tuple-element.13.refs_1_, ...), custom_call_target="tpu_custom_call" | custom-call | tf_op jit(solution)/shard_map/pallas_call | solution.py:443

commit v4 on v3

--- a/solution.py
+++ b/solution.py
@@ -48,8 +48,8 @@
 def kernel(
     tokens_hbm, gain_hbm, gate_hbm, up_hbm, down_hbm,
     gate_out, up_out, down_out, mixed_out,
-    tok, gain_in, gate_in, up_in, down_in, packed, r1, r2, w, normed, tok_send, tok_all, acc, core_send, core_got, plane_send, plane_got, db, parts, got, pieces, got2, last, mix,
-    in_sem, ts, tr, us, ur, vs, vr, xs, xr, as_, ar, bs, br, ds, dr, gs, gr, cs, cr, es, er, ps, pr, qs, qr, fs, fr,
+    tok, gain_in, gate_in, up_in, down_in, packed, r1, r2, w, normed, tok_send, tok_all, acc, core_send, core_got, plane_send, plane_got, db, cols_of, parts, got, pieces, got2,
+    in_sem, ts, tr, us, ur, vs, vr, xs, xr, as_, ar, bs, br, ds, dr, gs, gr, cs, cr, es, er, ps, pr, qs, qr,
 ):
     z, y, c, x = (lax.axis_index(a) for a in AXES)
     right, left, opposite = lax.rem(x + 1, 4), lax.rem(x + 3, 4), lax.rem(x + 2, 4)
@@ -69,11 +69,16 @@
     def second_peer(p):
         return (jnp.where(c == 0, p, z), jnp.where(c == 0, y, p), c, x)
 
+    def other_core(device):
+        return device[0], device[1], 1 - c, x
+
     barrier = pltpu.get_barrier_semaphore()
     peers = [x_peer(lax.rem(x + k, 4)) for k in (1, 2, 3)]
     peers += [first_peer(lax.rem(first + k, 8)) for k in range(1, 8)]
     peers += [second_peer(lax.rem(second + k, 8)) for k in range(1, 8)]
     peers += [partner]
+    peers += [other_core(second_peer(lax.rem(second + k, 8))) for k in range(1, 8)]
+    peers += [other_core(first_peer(lax.rem(first + k, 8))) for k in range(1, 8)]
     loads = [
         pltpu.make_async_copy(gate_hbm, gate_in, in_sem.at[0]),
         pltpu.make_async_copy(up_hbm, up_in, in_sem.at[1]),
@@ -103,7 +108,7 @@
             for n in range(3):
                 packed[n, s, j // 8, j % 8] = unit[:, 128 * n : 128 * n + 128]
 
-    pl.semaphore_wait(barrier, 18)
+    pl.semaphore_wait(barrier, 32)
     x_sends = []
     for n in range(3):
         x_sends.append([])
@@ -265,6 +270,22 @@
             go(gather_copy(x, n, 1, 2, right)), go(gather_copy(x, n, 0, 3, left)),
         ])
         swaps.append([go(core_copy(x, n, 0))])
+    land(whole)
+
+    @pl.when(c == 0)
+    def _():
+        for p in range(8):
+            cols = [
+                db[:, q // 2, :, :, 512 * (q % 2) + 64 * p : 512 * (q % 2) + 64 * p + 64].reshape(176, 64)
+                for q in range(8)
+            ]
+            cols_of[p] = jnp.concatenate(cols, axis=1)
+
+    @pl.when(c == 1)
+    def _():
+        for p in range(8):
+            cols_of[p] = db[:, p // 2, :, :, 512 * (p % 2) : 512 * (p % 2) + 512].reshape(176, 512)
+
     sums = []
     for n in range(3):
         for send in v_sends[n]:
@@ -276,27 +297,13 @@
     gate = jnp.concatenate([sums[0], sums[1][:, :48]], axis=1)
     up = jnp.concatenate([sums[1][:, 48:], sums[2][:, :96]], axis=1)
     hidden = (gate * (1.0 / (1.0 + jnp.exp(-gate))) * up).astype(BF16)
-    land(whole)
-
-    @pl.when(c == 0)
-    def _():
-        for p in range(8):
-            cols = [
-                db[:, q // 2, :, :, 512 * (q % 2) + 64 * p : 512 * (q % 2) + 64 * p + 64].reshape(176, 64)
-                for q in range(8)
-            ]
-            parts[p] = jnp.dot(hidden, jnp.concatenate(cols, axis=1), preferred_element_type=F32).astype(BF16)
-
-    @pl.when(c == 1)
-    def _():
-        for p in range(8):
-            cols = db[:, p // 2, :, :, 512 * (p % 2) : 512 * (p % 2) + 512].reshape(176, 512)
-            parts[p] = jnp.dot(hidden, cols, preferred_element_type=F32).astype(BF16)
 
     p_sends = []
-    for k in FAR_FIRST:
+    for k in (*FAR_FIRST, 0):
         p = lax.rem(first + k, 8)
-        p_sends.append(go(remote(parts.at[p], got.at[first], ps.at[k], pr.at[k], first_peer(p))))
+        parts[p] = jnp.dot(hidden, cols_of[p], preferred_element_type=F32).astype(BF16)
+        if k:
+            p_sends.append(go(remote(parts.at[p], got.at[first], ps.at[k], pr.at[k], first_peer(p))))
 
     for t in range(4):
         down_out[:, :, 1024 * t : 1024 * t + 1024] = db[c, t]
@@ -310,18 +317,24 @@
         land(ways[n][3])
         swaps[n].append(go(core_copy(right, n, 2)))
 
-    for send in p_sends:
+    q_sends = []
+    total = parts[first].astype(F32)
+    for k, send in zip(FAR_FIRST, p_sends):
         land(send)
-    total = parts[first].astype(F32)
-    for k in FAR_FIRST:
-        total += got[lax.rem(first + k, 8)].astype(F32)
-    for q in range(8):
-        both = jnp.concatenate([total[:48, 64 * q : 64 * q + 64], total[48:, 64 * q : 64 * q + 64]], axis=1)
-        pieces[q] = both.astype(BF16)
-    q_sends = []
-    for k in FAR_FIRST:
+        total += got[lax.rem(first + 8 - k, 8)].astype(F32)
+    for q in range(16):
+        groups = [total[32 * g : 32 * g + 32, 32 * q : 32 * q + 32] for g in range(3)]
+        block = jnp.concatenate(groups + [jnp.zeros((32, 32), F32)], axis=1)
+        pieces[q // 2, q % 2] = block.astype(BF16)
+    for k in (*FAR_FIRST, 0):
         p = lax.rem(second + k, 8)
-        q_sends.append(go(remote(pieces.at[p], got2.at[second], qs.at[k], qr.at[k], second_peer(p))))
+        for other in range(2):
+            if k or other:
+                d = 1 - c if other else c
+                device = other_core(second_peer(p)) if other else second_peer(p)
+                sems = qs.at[other, k], qr.at[other, k]
+                q_sends.append(go(remote(pieces.at[p, d], got2.at[c, second], *sems, device)))
+    got2[c, second] = pieces[second, c]
     for n in range(3):
         land(ways[n][4])
         land(ways[n][5])
@@ -345,23 +358,13 @@
                 lax.fori_loop(0, 8, unpack, 0)
     for send in q_sends:
         land(send)
-    total = pieces[second].astype(F32)
-    for k in FAR_FIRST:
-        total += got2[lax.rem(second + k, 8)].astype(F32)
-    total = jnp.concatenate([total[:, :64], total[:, 64:]], axis=0)
-
-    @pl.when(c == 0)
-    def _():
-        mix[c] = total[:, :32].astype(BF16)
-        last[...] = total[:, 32:].astype(BF16)
-
-    @pl.when(c == 1)
-    def _():
-        mix[c] = total[:, 32:].astype(BF16)
-        last[...] = total[:, :32].astype(BF16)
-
-    land(go(remote(last, mix.at[c], fs, fr, partner)))
-    mixed_out[...] = jnp.concatenate([mix[0], mix[1]], axis=0).astype(F32).T.astype(BF16)
+    blocks = []
+    for core in range(2):
+        total = got2[core, 0].astype(F32)
+        for q in range(1, 8):
+            total += got2[core, q].astype(F32)
+        blocks += [total[:, 32 * g : 32 * g + 32] for g in range(3)]
+    mixed_out[...] = jnp.concatenate(blocks, axis=0).T.astype(BF16)
     flights.finish()
 
 
@@ -409,12 +412,11 @@
             vmem((3, 4, 96, 128), BF16),
             vmem((3, 4, 96, 128), BF16),
             vmem((2, 4, 11, 8, 1024), BF16),
+            vmem((8, 176, 512), BF16),
             vmem((8, 96, 512), BF16),
             vmem((8, 96, 512), BF16),
-            vmem((8, 48, 128), BF16),
-            vmem((8, 48, 128), BF16),
-            vmem((96, 32), BF16),
-            vmem((2, 96, 32), BF16),
+            vmem((8, 2, 32, 128), BF16),
+            vmem((2, 8, 32, 128), BF16),
             dma((5,)),
             dma((4,)), dma((4,)),
             dma((3,)), dma((3,)),
@@ -427,8 +429,7 @@
             dma((3, 4)), dma((3, 4)),
             dma, dma,
             dma((8,)), dma((8,)),
-            dma((8,)), dma((8,)),
-            dma, dma,
+            dma((2, 8)), dma((2, 8)),
         ],
         compiler_params=pltpu.CompilerParams(
             collective_id=0, has_side_effects=True, vmem_limit_bytes=LIMIT

time: 64.9 us -> 63.9 us (0.985)
  Pallas kernels: 64.1 us -> 63.1 us
    pallas_call x1, Pallas kernels: 62.7 us -> 61.8 us  [on_device(): pl.pallas_call(kernel, out_shape=[pltpu.VMEM(a.shape, a.dtype) for a in s...]
where the time goes in v4:
time: 63.9 us; the launch traced here: 63.8 us
  Pallas kernels  63.1 us (99%)
  between operations  0.64 us (1%)
    pallas_call x1, Pallas kernels, on_device(): pl.pallas_call(kernel, out_shape=[pltpu.VMEM(a.shape, a.dtype) for a in s...  61.8 us
    pallas_call x1, Pallas kernels, on_device(): pl.pallas_call(write_out, out_shape=shapes, in_specs=[in_vmem] * 4, out_s...  1.37 us

profile of v4, /device:TPU:1, one launch (start us, length us, event | category | flops | bytes accessed | tf_op | source)
XLA Modules:
  0.0 63.8 jit_solution(11568722834522123311)
XLA Ops:
  0.6 61.8 %shard_map.84 = (bf16[11,8,4096]{2,1,0:T(8,128)(2,1)S(1)}, bf16[11,8,4096]{2,1,0:T(8,128)(2,1)S(1)}, bf16[11,8,4096]{2,1,0:T(8,128)(2,1)S(1)}, bf16[32,192]{1,0:T(8,128)(2,1)S(1)}) custom-call(bf16[192,4096]{1,0:T(8,128)(2,1)} %tokens_hbm.1, f32[1,32]{1,0:T(1,128)} %bitcast.9, f32[32,2816]{1,0:T(8,128)} %gate_hbm.1, f32[32,2816]{1,0:T(8,128)} %up_hbm.1, ...), custom_call_target="tpu_custom_call" | custom-call | tf_op jit(solution)/shard_map/pallas_call | solution.py:391
  62.4 1.4 %shard_map.85 = (bf16[11,8,4096]{2,1,0:T(8,128)(2,1)}, bf16[11,8,4096]{2,1,0:T(8,128)(2,1)}, bf16[11,8,4096]{2,1,0:T(8,128)(2,1)}, bf16[32,192]{1,0:T(8,128)(2,1)}) custom-call(bf16[11,8,4096]{2,1,0:T(8,128)(2,1)S(1)} %get-tuple-element.12.refs_0_, bf16[11,8,4096]{2,1,0:T(8,128)(2,1)S(1)} %get-tuple-element.13.refs_1_, ...), custom_call_target="tpu_custom_call" | custom-call | tf_op jit(solution)/shard_map/pallas_call | solution.py:444

commit v5 on v4

--- a/solution.py
+++ b/solution.py
@@ -86,8 +86,8 @@
         pltpu.make_async_copy(tokens_hbm, tok, in_sem.at[3]),
         pltpu.make_async_copy(gain_hbm, gain_in, in_sem.at[4]),
     ]
-    for load in loads:
-        load.start()
+    for k in (0, 4, 1):
+        loads[k].start()
     for peer in peers:
         pl.semaphore_signal(barrier, inc=1, device_id=peer, device_id_type=MESH)
 
@@ -97,20 +97,30 @@
     spread = jnp.broadcast_to(gain_in[...], (32, 32))
     gain = jnp.sum(jnp.where(lanes == rows, spread, 0.0), axis=1, keepdims=True)
     loads[0].wait()
-    loads[1].wait()
-    for s in range(4):
-        scale = gain[8 * s : 8 * s + 8]
-        g = gate_in[8 * s : 8 * s + 8, :] * scale
-        u = up_in[8 * s : 8 * s + 8, :] * scale
-        for j in range(16):
-            cut = slice(176 * j, 176 * j + 176)
-            unit = jnp.concatenate([g[:, cut], u[:, cut], jnp.zeros((8, 32), F32)], axis=1).astype(BF16)
-            for n in range(3):
-                packed[n, s, j // 8, j % 8] = unit[:, 128 * n : 128 * n + 128]
-
-    pl.semaphore_wait(barrier, 32)
+    loads[2].start()
+    loads[3].start()
+
+    def scaled(ref, s):
+        return ref[8 * s : 8 * s + 8, :] * gain[8 * s : 8 * s + 8]
+
     x_sends = []
     for n in range(3):
+        if n == 1:
+            loads[1].wait()
+        for s in range(4):
+            g = scaled(gate_in, s) if n < 2 else None
+            u = scaled(up_in, s) if n > 0 else None
+            for j in range(16):
+                at = 176 * j
+                if n == 0:
+                    tile = g[:, at : at + 128]
+                elif n == 1:
+                    tile = jnp.concatenate([g[:, at + 128 : at + 176], u[:, at : at + 80]], axis=1)
+                else:
+                    tile = jnp.concatenate([u[:, at + 80 : at + 176], jnp.zeros((8, 32), F32)], axis=1)
+                packed[n, s, j // 8, j % 8] = tile.astype(BF16)
+        if n == 0:
+            pl.semaphore_wait(barrier, 32)
         x_sends.append([])
         for k in (2, 1, 3):
             p = lax.rem(x + k, 4)

time: 63.9 us -> 64.1 us (level)
  no operation moved by 1% of the time
where the time goes in v5:
time: 64.1 us; the launch traced here: 64 us
  Pallas kernels  63.3 us (99%)
    pallas_call x1, Pallas kernels, on_device(): pl.pallas_call(kernel, out_shape=[pltpu.VMEM(a.shape, a.dtype) for a in s...  62 us
    pallas_call x1, Pallas kernels, on_device(): pl.pallas_call(write_out, out_shape=shapes, in_specs=[in_vmem] * 4, out_s...  1.37 us

profile of v5, /device:TPU:1, one launch (start us, length us, event | category | flops | bytes accessed | tf_op | source)
XLA Modules:
  0.0 64.0 jit_solution(2782218929440785101)
XLA Ops:
  0.6 62.0 %shard_map.84 = (bf16[11,8,4096]{2,1,0:T(8,128)(2,1)S(1)}, bf16[11,8,4096]{2,1,0:T(8,128)(2,1)S(1)}, bf16[11,8,4096]{2,1,0:T(8,128)(2,1)S(1)}, bf16[32,192]{1,0:T(8,128)(2,1)S(1)}) custom-call(bf16[192,4096]{1,0:T(8,128)(2,1)} %tokens_hbm.1, f32[1,32]{1,0:T(1,128)} %bitcast.9, f32[32,2816]{1,0:T(8,128)} %gate_hbm.1, f32[32,2816]{1,0:T(8,128)} %up_hbm.1, ...), custom_call_target="tpu_custom_call" | custom-call | tf_op jit(solution)/shard_map/pallas_call | solution.py:401
  62.6 1.4 %shard_map.85 = (bf16[11,8,4096]{2,1,0:T(8,128)(2,1)}, bf16[11,8,4096]{2,1,0:T(8,128)(2,1)}, bf16[11,8,4096]{2,1,0:T(8,128)(2,1)}, bf16[32,192]{1,0:T(8,128)(2,1)}) custom-call(bf16[11,8,4096]{2,1,0:T(8,128)(2,1)S(1)} %get-tuple-element.12.refs_0_, bf16[11,8,4096]{2,1,0:T(8,128)(2,1)S(1)} %get-tuple-element.13.refs_1_, ...), custom_call_target="tpu_custom_call" | custom-call | tf_op jit(solution)/shard_map/pallas_call | solution.py:454

commit v6 on v4

--- a/solution.py
+++ b/solution.py
@@ -158,6 +158,11 @@
         go(down_copy(x, 1, 2, right)), go(down_copy(x, 0, 3, left)),
     ]
 
+    def down_swap(t, k):
+        return remote(db.at[c, t], db.at[c, t], es.at[k], er.at[k], partner)
+
+    d_swaps = [go(down_swap(x, 0))]
+
     for n in range(3):
         r1[n, pl.ds(2 * x, 2)] = packed[n, x]
 
@@ -249,6 +254,10 @@
             d_ways.append(go(down_copy(left, 0, 4, right)))
             land(d_ways[1])
             d_ways.append(go(down_copy(right, 1, 5, left)))
+            land(d_ways[2])
+            d_swaps.append(go(down_swap(left, 1)))
+            land(d_ways[3])
+            d_swaps.append(go(down_swap(right, 2)))
     v_sends = []
     for n in range(3):
         land(u_sends[n])
@@ -259,9 +268,9 @@
             v_sends[n].append(
                 go(remote(plane_send.at[n, p], plane_got.at[n, x], vs.at[n, k], vr.at[n, k], x_peer(p)))
             )
-    for send in d_ways[2:]:
+    for send in d_ways[4:]:
         land(send)
-    whole = go(remote(db.at[c], db.at[c], es, er, partner))
+    d_swaps.append(go(down_swap(opposite, 3)))
     ways = []
     swaps = []
     for n in range(3):
@@ -270,7 +279,8 @@
             go(gather_copy(x, n, 1, 2, right)), go(gather_copy(x, n, 0, 3, left)),
         ])
         swaps.append([go(core_copy(x, n, 0))])
-    land(whole)
+    for send in d_swaps:
+        land(send)
 
     @pl.when(c == 0)
     def _():
@@ -427,7 +437,7 @@
             dma((6,)), dma((6,)),
             dma((3, 6)), dma((3, 6)),
             dma((3, 4)), dma((3, 4)),
-            dma, dma,
+            dma((4,)), dma((4,)),
             dma((8,)), dma((8,)),
             dma((2, 8)), dma((2, 8)),
         ],

time: 63.9 us -> 64 us (level)
  no operation moved by 1% of the time
where the time goes in v6:
time: 64 us; the launch traced here: 63.9 us
  Pallas kernels  63.2 us (99%)
  between operations  0.64 us (1%)
    pallas_call x1, Pallas kernels, on_device(): pl.pallas_call(kernel, out_shape=[pltpu.VMEM(a.shape, a.dtype) for a in s...  61.8 us
    pallas_call x1, Pallas kernels, on_device(): pl.pallas_call(write_out, out_shape=shapes, in_specs=[in_vmem] * 4, out_s...  1.37 us

profile of v6, /device:TPU:1, one launch (start us, length us, event | category | flops | bytes accessed | tf_op | source)
XLA Modules:
  0.0 63.9 jit_solution(9961387281569774422)
XLA Ops:
  0.6 61.8 %shard_map.84 = (bf16[11,8,4096]{2,1,0:T(8,128)(2,1)S(1)}, bf16[11,8,4096]{2,1,0:T(8,128)(2,1)S(1)}, bf16[11,8,4096]{2,1,0:T(8,128)(2,1)S(1)}, bf16[32,192]{1,0:T(8,128)(2,1)S(1)}) custom-call(bf16[192,4096]{1,0:T(8,128)(2,1)} %tokens_hbm.1, f32[1,32]{1,0:T(1,128)} %bitcast.9, f32[32,2816]{1,0:T(8,128)} %gate_hbm.1, f32[32,2816]{1,0:T(8,128)} %up_hbm.1, ...), custom_call_target="tpu_custom_call" | custom-call | tf_op jit(solution)/shard_map/pallas_call | solution.py:401
  62.5 1.4 %shard_map.85 = (bf16[11,8,4096]{2,1,0:T(8,128)(2,1)}, bf16[11,8,4096]{2,1,0:T(8,128)(2,1)}, bf16[11,8,4096]{2,1,0:T(8,128)(2,1)}, bf16[32,192]{1,0:T(8,128)(2,1)}) custom-call(bf16[11,8,4096]{2,1,0:T(8,128)(2,1)S(1)} %get-tuple-element.12.refs_0_, bf16[11,8,4096]{2,1,0:T(8,128)(2,1)S(1)} %get-tuple-element.13.refs_1_, ...), custom_call_target="tpu_custom_call" | custom-call | tf_op jit(solution)/shard_map/pallas_call | solution.py:454
